TPU v7x, 32 devices: a whole 2x2x4 slice. The times are simulated.
32 devices in a mesh: rep: 2 (over x), fs: 8 (over z, y), tp: 2 (over core).
Axes of the slice: x: 2, y: 2, z: 4, core: 2. Of those that a mesh axis runs over, the one named last changes fastest.
Arguments:
- inputs: bfloat16 [2, 3072, 2048], P('rep', 'fs', 'tp'), may hold values from -6 to 6
- gate_proj: bfloat16 [2048, 2816], P('fs', 'tp'), may hold values from -0.125 to 0.125
- value_proj: bfloat16 [2048, 2816], P('fs', 'tp'), may hold values from -0.125 to 0.125
- gate_taps: float32 [3, 2816], replicated, may hold values from -3 to 3
- value_taps: float32 [3, 2816], replicated, may hold values from -3 to 3
- out_grad: bfloat16 [2, 3072, 2816], P('rep', 'fs', 'tp'), may hold values from -6 to 6
Outputs:
- in_grad: bfloat16 [2, 3072, 2048], P('rep', 'fs', 'tp')
- gate_proj_grad: float32 [2048, 2816], P('fs', 'tp')
- value_proj_grad: float32 [2048, 2816], P('fs', 'tp')
- gate_taps_grad: float32 [3, 2816], replicated
- value_taps_grad: float32 [3, 2816], replicated
All inputs are finite; a program needn't handle non-finite values.
Results may differ from a plain program's by a relative error of at most 0.013.
Values may be sent and summed in bfloat16 or wider, within the bound.
A program may use at most 128 MiB of HBM per device.

v0:
```python
import jax
import jax.numpy as jnp
from jax import lax
from jax.sharding import PartitionSpec as P

HALO = 8


def shift(x, axis, step):
    count = lax.axis_size(axis)
    return lax.ppermute(x, axis, [(i, (i + step) % count) for i in range(count)])


def with_halo(rows):
    count = lax.axis_size("fs")
    nxt = lax.ppermute(rows[:HALO], "fs", [(i + 1, i) for i in range(count - 1)])
    prv = lax.ppermute(rows[rows.shape[0] - HALO :], "fs", [(i, i + 1) for i in range(count - 1)])
    return jnp.concatenate([rows, nxt, prv], axis=0)


def before(x):
    return jnp.concatenate([x[:, -1:], x[:, :-1]], axis=1)


def after(x):
    return jnp.concatenate([x[:, 1:], x[:, :1]], axis=1)


def shards(inputs, gate_proj, value_proj, gate_taps, value_taps, out_grad):
    contract_cols = (((1,), (1,)), ((), ()))
    contract_rows = (((0,), (0,)), ((), ()))
    reps, fs_count = (lax.axis_size("rep"), lax.axis_size("fs"))
    rep = lax.axis_index("rep")
    tokens, feats = inputs.shape[1:]
    hid = gate_proj.shape[1]
    width = min(hid, -(-hid // reps // 128) * 128)
    last = hid - width

    def start_of(part):
        return jnp.minimum(part * width, last)

    first = start_of(rep)
    dead = rep * width - first
    live = jnp.arange(width) >= dead

    def part_cols(x, part):
        return lax.dynamic_slice_in_dim(x, start_of(part), width, x.ndim - 1)

    w_own = jnp.concatenate(
        [
            jnp.where(live, part_cols(w, rep), jnp.zeros((), w.dtype))
            for w in (gate_proj, value_proj)
        ],
        axis=1,
    )
    w_all = lax.all_gather(w_own, "fs", axis=0, tiled=True)
    x_ext = with_halo(inputs[0])
    g_ext = with_halo(out_grad[0])
    x_blocks, g_blocks = ([x_ext], [part_cols(g_ext, rep)])
    for step in range(1, reps):
        x_blocks.append(shift(x_ext, "rep", step))
        g_blocks.append(shift(part_cols(g_ext, (rep + step) % reps), "rep", step))
    x_all = lax.all_gather(jnp.stack(x_blocks), "tp", axis=2, tiled=True)
    g_all = jnp.stack(g_blocks).astype(jnp.float32)
    ext = tokens + 2 * HALO
    pre = jnp.dot(x_all.reshape(reps * ext, -1), w_all, preferred_element_type=jnp.float32)
    pre = pre.astype(jnp.bfloat16).astype(jnp.float32).reshape(reps, ext, 2 * width)
    tap_start = lax.axis_index("tp") * hid + first
    taps = jnp.concatenate(
        [lax.dynamic_slice_in_dim(t, tap_start, width, 1) for t in (gate_taps, value_taps)], axis=1
    )
    pre_b, pre_a = (before(pre), after(pre))
    mix = taps[0] * pre_b + taps[1] * pre + taps[2] * pre_a
    gate_mix, value_mix = (mix[..., :width], mix[..., width:])
    sig = jax.nn.sigmoid(gate_mix)
    gate_cot = g_all * value_mix * (sig * (1.0 + gate_mix * (1.0 - sig)))
    value_cot = g_all * (gate_mix * sig)
    cot = jnp.concatenate([gate_cot, value_cot], axis=2)
    pre_cot = taps[0] * after(cot) + taps[1] * cot + taps[2] * before(cot)
    pre_cot = pre_cot[:, :tokens].astype(jnp.bfloat16).reshape(reps * tokens, 2 * width)
    tap_terms = jnp.stack(
        [jnp.sum(p[:, :tokens] * cot[:, :tokens], axis=(0, 1)) for p in (pre_b, pre, pre_a)]
    )
    factor = float(tokens * fs_count * reps) ** (-0.5)
    grads = lax.dot_general(
        x_all[:, :tokens].reshape(reps * tokens, -1),
        pre_cot,
        contract_rows,
        preferred_element_type=jnp.float32,
    )
    grads = (grads * factor).astype(jnp.bfloat16)
    own = lax.psum_scatter(grads, "fs", scatter_dimension=0, tiled=True)
    partial_value = lax.dot_general(
        pre_cot, w_all, contract_cols, preferred_element_type=jnp.float32
    )
    partial_value = lax.psum_scatter(
        partial_value.astype(jnp.bfloat16), "tp", scatter_dimension=1, tiled=True
    ).reshape(reps, tokens, feats)
    in_grad = partial_value[0].astype(jnp.float32)
    for step in range(1, reps):
        in_grad += shift(partial_value[step], "rep", -step).astype(jnp.float32)
    blocks = [own]
    for step in range(1, reps):
        blocks.append(shift(own, "rep", step))
    proj_grads = []
    for branch in range(2):
        cols = jnp.zeros((own.shape[0], hid), jnp.bfloat16)
        cut = [b[:, branch * width : (branch + 1) * width] for b in blocks]
        for step in range(reps):
            part = (rep - step) % reps
            place = start_of(part)
            skip = part * width - place
            old = lax.dynamic_slice_in_dim(cols, place, width, 1)
            new = jnp.where(jnp.arange(width) >= skip, cut[step], old)
            cols = lax.dynamic_update_slice_in_dim(cols, new, place, 1)
        proj_grads.append(cols.astype(jnp.float32))
    tap_sum = lax.psum(tap_terms * factor, "fs").reshape(3, 2, width)
    tap_all = lax.all_gather(lax.all_gather(tap_sum, "rep"), "tp")
    halves = []
    for half in range(tap_all.shape[0]):
        cols = [
            tap_all[half, p, :, :, max(0, p * width - last) if p * width > last else 0 :]
            for p in range(reps)
        ]
        halves.append(jnp.concatenate(cols, axis=2))
    taps_out = jnp.concatenate(halves, axis=2)
    return (
        in_grad.astype(jnp.bfloat16)[None],
        proj_grads[0],
        proj_grads[1],
        taps_out[:, 0],
        taps_out[:, 1],
    )


def solution(mesh):
    placed = (P("rep", "fs", "tp"), P("fs", "tp"), P("fs", "tp"), P(), P(), P("rep", "fs", "tp"))
    return jax.shard_map(
        shards,
        mesh=mesh,
        in_specs=placed,
        out_specs=(P("rep", "fs", "tp"), P("fs", "tp"), P("fs", "tp"), P(), P()),
        check_vma=False,
    )
```

profile of v0, /device:TPU:2, one launch (start us, length us, event | category | flops | bytes accessed | tf_op | source)
XLA Modules:
  0.0 368.1 jit_solution(3353467001362223861)
XLA Ops:
  7.2 1.5 copy.18
  8.8 3.4 collective-permute-start.4
  12.3 1.3 collective-permute-start.3
  13.6 9.8 %collective-permute-done.4 = bf16[8,1024]{0,1:T(8,128)(2,1)S(1)} collective-permute-done((bf16[8,1024]{0,1:T(8,128)(2,1)S(1)}, bf16[8,1024]{0,1:T(8,128)(2,1)S(1)}, u32[]{:S(2)}, u32[]{:S(2)}) %collective-permute-start.4) | collective-permute-done | bytes 16416 | tf_op jit(solution)/shard_map/ppermute | solution.py:17
  24.9 16.7 %collective-permute-done.5 = bf16[400,1024]{1,0:T(8,128)(2,1)} collective-permute-done((bf16[400,1024]{1,0:T(8,128)(2,1)S(1)}, bf16[400,1024]{1,0:T(8,128)(2,1)}, u32[]{:S(2)}, u32[]{:S(2)}) %collective-permute-start.5) | collective-permute-done | bytes 819232 | tf_op jit(solution)/shard_map/ppermute | solution.py:11
  41.6 1.4 copy.22
  43.1 1.6 pad_maximum_fusion.4
  44.8 1.5 dynamic-slice_select_fusion.1
  47.3 6.2 %collective-permute-start.1 = (bf16[8,1408]{1,0:T(8,128)(2,1)S(1)}, bf16[8,1408]{1,0:T(8,128)(2,1)S(1)}, u32[]{:S(2)}, u32[]{:S(2)}) collective-permute-start(bf16[8,1408]{1,0:T(8,128)(2,1)S(1)} %get-tuple-element.25), channel_id=1, source_target_pairs={{0,2},{2,4},{4,6},{6,8},{8,10},{10,12},{12,14},{1,3},{3,5},{5,7},{... | collective-permute-start | bytes 67592 | tf_op jit(solution)/shard_map/ppermute | solution.py:17
  53.5 1.5 collective-permute-start
  55.9 4.8 %collective-permute-done = bf16[8,1408]{1,0:T(8,128)(2,1)S(1)} collective-permute-done((bf16[8,1408]{1,0:T(8,128)(2,1)S(1)}, bf16[8,1408]{1,0:T(8,128)(2,1)S(1)}, u32[]{:S(2)}, u32[]{:S(2)}) %collective-permute-start) | collective-permute-done | bytes 22560 | tf_op jit(solution)/shard_map/ppermute | solution.py:16
  60.7 1.6 dynamic-slice_bitcast_fusion
  63.7 4.7 %copy.23 = bf16[2,400,2048]{2,1,0:T(8,128)(2,1)S(1)} copy(bf16[2,400,2048]{1,2,0:T(8,128)(2,1)} %all-gather.4.cloned.1.call-done) | data formatting | bytes 6553600 | tf_op jit(solution)/shard_map/all_gather | solution.py:63
  68.4 97.7 %all-gather.6.cloned.1.call-done = bf16[2048,1536]{1,0:T(8,128)(2,1)} async-done(((bf16[256,1536]{1,0:T(8,128)(2,1)}), bf16[2048,1536]{1,0:T(8,128)(2,1)}) %all-gather.6.cloned.1.call-update) | async-done | bytes 6291472 | tf_op jit(solution)/shard_map/all_gather | solution.py:56
  166.1 8.2 %convolution_convert_fusion = bf16[800,1536]{1,0:T(8,128)(2,1)S(1)} fusion(bf16[800,2048]{1,0:T(8,128)(2,1)S(1)} %bitcast.55, bf16[2048,1536]{1,0:T(8,128)(2,1)} %all-gather.6.cloned.1.call-done), kind=kOutput, calls=%fused_computation.37 | convolution fusion | flops 5034393600 | bytes 12025856 | tf_op jit(solution)/shard_map/dot_general | solution.py:66
  175.0 1.3 fusion.24
  176.3 1.7 fusion.3
  178.0 2.2 convert_multiply_fusion
  181.3 8.2 %fusion.15 = (f32[1536]{0:T(1024)S(1)}, f32[1536]{0:T(1024)S(1)}, f32[1536]{0:T(1024)S(1)}, bf16[2,384,1536]{2,1,0:T(8,128)(2,1)S(1)}) fusion(f32[2,400,1536]{2,1,0:T(8,128)S(1)} %convert.5, f32[2,400,768]{2,1,0:T(8,128)S(1)} %get-tuple-element.11, f32[2,400,768]{2,1,0:T(8,128)S(1)} %get-tuple-element.12, f32[2,399,1536]{2,1,0:T(8,128)S(1)} %get-tuple-element.18, ...), kind=kLoop, calls=%fused_computation.31 | loop fusion | flops 20049408 | bytes 31494144 | tf_op jit(solution)/shard_map/reduce_sum | solution.py:82
  189.6 9.3 %convolution_convert_fusion.1 = bf16[768,2048]{1,0:T(8,128)(2,1)} fusion(bf16[768,1536]{1,0:T(8,128)(2,1)S(1)} %bitcast.56, bf16[2048,1536]{1,0:T(8,128)(2,1)} %all-gather.6.cloned.1.call-done), kind=kOutput, calls=%fused_computation.38 | convolution fusion | flops 4833411072 | bytes 11796480 | tf_op jit(solution)/shard_map/dot_general | solution.py:93
  199.2 8.9 %fusion = bf16[2048,1536]{1,0:T(8,128)(2,1)} fusion(bf16[2,384,1536]{2,1,0:T(8,128)(2,1)S(1)} %get-tuple-element.13, bf16[2,400,2048]{1,2,0:T(8,128)(2,1)} %all-gather.4.cloned.1.call-done), kind=kOutput, calls=%fused_computation.1 | convolution fusion | flops 4838129664 | bytes 11796480 | tf_op jit(solution)/shard_map/dot_general | solution.py:85
  208.3 35.4 %psum.7 = f32[1,3,2,768]{3,2,1,0:T(2,128)S(1)} all-reduce(f32[1,3,2,768]{3,2,1,0:T(2,128)S(1)} %all_gather_reshape.3), channel_id=1, replica_groups=mesh['rep'=2,'fs'=8,'tp'=2] {'fs'}, use_global_device_ids=true, to_apply=%region_5.6 | all-reduce | flops 4608 | bytes 36864 | tf_op jit(solution)/shard_map/psum | solution.py:117
  243.7 4.4 %all_gather.17 = f32[2,3,2,768]{3,2,1,0:T(2,128)S(1)} all-gather(f32[1,3,2,768]{3,2,1,0:T(2,128)S(1)} %psum.7), channel_id=1, replica_groups=mesh['rep'=2,'fs'=8,'tp'=2] {'rep'}, dimensions={0}, use_global_device_ids=true | all-gather | bytes 55296 | tf_op jit(solution)/shard_map/all_gather | solution.py:118
  248.1 1.8 all-gather
  250.0 1.2 slice.184
  252.1 79.1 %reduce-scatter.5.cloned.1.call-done = bf16[256,1536]{1,0:T(8,128)(2,1)} async-done(((bf16[2048,1536]{1,0:T(8,128)(2,1)}), bf16[256,1536]{1,0:T(8,128)(2,1)}) %reduce-scatter.5.cloned.1.call-update) | async-done | bytes 786448 | tf_op jit(solution)/shard_map/reduce_scatter | solution.py:92
  332.4 2.3 fusion.20
  336.0 3.1 dynamic_update_slice.12
  339.2 3.1 dynamic_update_slice.14
  342.3 7.6 %collective-permute-done.7 = bf16[256,1536]{1,0:T(8,128)(2,1)S(1)} collective-permute-done((bf16[256,1536]{1,0:T(8,128)(2,1)}, bf16[256,1536]{1,0:T(8,128)(2,1)S(1)}, u32[]{:S(2)}, u32[]{:S(2)}) %collective-permute-start.7) | collective-permute-done | bytes 786464 | tf_op jit(solution)/shard_map/ppermute | solution.py:11
  350.4 4.4 %dynamic_update_slice.13 = bf16[256,1408]{1,0:T(8,128)(2,1)S(1)} dynamic-update-slice(bf16[256,1408]{1,0:T(8,128)(2,1)S(1)} %dynamic_update_slice.12, bf16[256,768]{1,0:T(8,128)(2,1)S(1)} %get-tuple-element.27, s32[]{:T(128)} %constant.42.clone.1, s32[]{:T(128)S(6)} %select_n.71) | dynamic-update-slice | bytes 786436 | tf_op jit(solution)/shard_map/dynamic_update_slice | solution.py:115
  356.0 4.3 %dynamic_update_slice.15 = bf16[256,1408]{1,0:T(8,128)(2,1)S(1)} dynamic-update-slice(bf16[256,1408]{1,0:T(8,128)(2,1)S(1)} %dynamic_update_slice.14, bf16[256,768]{1,0:T(8,128)(2,1)S(1)} %get-tuple-element.26, s32[]{:T(128)} %constant.42.clone.1, s32[]{:T(128)S(6)} %select_n.71) | dynamic-update-slice | bytes 786436 | tf_op jit(solution)/shard_map/dynamic_update_slice | solution.py:115
  (57 shorter events, 13.4 us)
Async XLA Ops:
  7.2 56.6 %all-gather.4.cloned.1.call-start = ((), (), s32[]{:S(2)}) async-start(), calls=%async_computation.2 | async-start | bytes 6291456 | tf_op jit(solution)/shard_map/all_gather | solution.py:63
  8.8 14.6 %collective-permute-start.4 = (bf16[8,1024]{0,1:T(8,128)(2,1)S(1)}, bf16[8,1024]{0,1:T(8,128)(2,1)S(1)}, u32[]{:S(2)}, u32[]{:S(2)}) collective-permute-start(bf16[8,1024]{0,1:T(8,128)(2,1)S(1)} %get-tuple-element.31), channel_id=1, source_target_pairs={{0,2},{2,4},{4,6},{6,8},{8,10},{10,12},{12,14},{1,3},{3,5},{5,7},{... | collective-permute-start | bytes 49160 | tf_op jit(solution)/shard_map/ppermute | solution.py:17
  12.3 11.2 %collective-permute-start.3 = (bf16[8,1024]{0,1:T(8,128)(2,1)S(1)}, bf16[8,1024]{0,1:T(8,128)(2,1)S(1)}, u32[]{:S(2)}, u32[]{:S(2)}) collective-permute-start(bf16[8,1024]{0,1:T(8,128)(2,1)S(1)} %get-tuple-element.30), channel_id=1, source_target_pairs={{2,0},{4,2},{6,4},{8,6},{10,8},{12,10},{14,12},{3,1},{5,3},{7,5},{... | collective-permute-start | bytes 49160 | tf_op jit(solution)/shard_map/ppermute | solution.py:16
  24.1 17.5 %collective-permute-start.5 = (bf16[400,1024]{1,0:T(8,128)(2,1)S(1)}, bf16[400,1024]{1,0:T(8,128)(2,1)}, u32[]{:S(2)}, u32[]{:S(2)}) collective-permute-start(bf16[400,1024]{1,0:T(8,128)(2,1)S(1)} %copy.21), channel_id=1, source_target_pairs={{0,16},{16,0},{1,17},{17,1},{2,18},{18,2},{3,19},{19,3},{4,20},{20... | collective-permute-start | bytes 2457608 | tf_op jit(solution)/shard_map/ppermute | solution.py:11
  43.1 4.2 %copy-start.1 = (bf16[1,384,1408]{2,1,0:T(8,128)(2,1)S(1)}, bf16[1,384,1408]{2,1,0:T(8,128)(2,1)}, u32[]{:S(2)}) copy-start(bf16[1,384,1408]{2,1,0:T(8,128)(2,1)} %param.11) | copy-start | bytes 3244036
  44.7 121.4 %all-gather.6.cloned.1.call-start = ((), (), s32[]{:S(2)}) async-start(), calls=%async_computation.3 | async-start | bytes 7077888 | tf_op jit(solution)/shard_map/all_gather | solution.py:56
  47.2 202.8 %reduce-scatter.3.cloned.1.call-start = ((), (), s32[]{:S(2)}) async-start(), calls=%async_computation.4 | async-start | bytes 4718592 | tf_op jit(solution)/shard_map/reduce_scatter | solution.py:96
  47.3 8.5 %collective-permute-start.1 = (bf16[8,1408]{1,0:T(8,128)(2,1)S(1)}, bf16[8,1408]{1,0:T(8,128)(2,1)S(1)}, u32[]{:S(2)}, u32[]{:S(2)}) collective-permute-start(bf16[8,1408]{1,0:T(8,128)(2,1)S(1)} %get-tuple-element.25), channel_id=1, source_target_pairs={{0,2},{2,4},{4,6},{6,8},{8,10},{10,12},{12,14},{1,3},{3,5},{5,7},{... | collective-permute-start | bytes 67592 | tf_op jit(solution)/shard_map/ppermute | solution.py:17
  53.5 7.1 %collective-permute-start = (bf16[8,1408]{1,0:T(8,128)(2,1)S(1)}, bf16[8,1408]{1,0:T(8,128)(2,1)S(1)}, u32[]{:S(2)}, u32[]{:S(2)}) collective-permute-start(bf16[8,1408]{1,0:T(8,128)(2,1)S(1)} %get-tuple-element.24), channel_id=1, source_target_pairs={{2,0},{4,2},{6,4},{8,6},{10,8},{12,10},{14,12},{3,1},{5,3},{7,5},{... | collective-permute-start | bytes 67592 | tf_op jit(solution)/shard_map/ppermute | solution.py:16
  62.3 115.7 %collective-permute-start.2 = (bf16[400,768]{1,0:T(8,128)(2,1)}, bf16[400,768]{1,0:T(8,128)(2,1)}, u32[]{:S(2)}, u32[]{:S(2)}) collective-permute-start(bf16[400,768]{1,0:T(8,128)(2,1)} %get-tuple-element.23), channel_id=1, source_target_pairs={{0,16},{16,0},{1,17},{17,1},{2,18},{18,2},{3,19},{19,3},{4,20},{20... | collective-permute-start | bytes 1843208 | tf_op jit(solution)/shard_map/ppermute | solution.py:11
  176.3 1.7 copy-start
  198.9 132.3 %reduce-scatter.5.cloned.1.call-start = ((), (), s32[]{:S(2)}) async-start(), calls=%async_computation.5 | async-start | bytes 7077888 | tf_op jit(solution)/shard_map/reduce_scatter | solution.py:92
  251.3 81.2 %collective-permute-start.6 = (bf16[384,1024]{1,0:T(8,128)(2,1)S(1)}, bf16[384,1024]{1,0:T(8,128)(2,1)S(1)}, u32[]{:S(2)}, u32[]{:S(2)}) collective-permute-start(bf16[384,1024]{1,0:T(8,128)(2,1)S(1)} %slice.184), channel_id=1, source_target_pairs={{0,16},{16,0},{1,17},{17,1},{2,18},{18,2},{3,19},{19,3},{4,20},{20... | collective-permute-start | bytes 2359304 | tf_op jit(solution)/shard_map/ppermute | solution.py:11
  331.2 18.7 %collective-permute-start.7 = (bf16[256,1536]{1,0:T(8,128)(2,1)}, bf16[256,1536]{1,0:T(8,128)(2,1)S(1)}, u32[]{:S(2)}, u32[]{:S(2)}) collective-permute-start(bf16[256,1536]{1,0:T(8,128)(2,1)} %reduce-scatter.5.cloned.1.call-done), channel_id=1, source_target_pairs={{0,16},{16,0},{1,17},{17,1},{2,18},{18,2},{3,19},{19,3},{4,20},{20... | collective-permute-start | bytes 2359304 | tf_op jit(solution)/shard_map/ppermute | solution.py:11
Sparse Core Ops, SparseCore 0:
  44.8 18.8 all-gather.3
  66.5 99.5 all-gather.5
  199.0 9.4 reduce-scatter.2
  212.0 119.1 reduce-scatter.4
where the time goes:
time: 369 us; the launch traced here: 368 us
  waiting for transfers between devices  217 us (59%)
  blocking collectives  41.6 us (11%)
  local copies, waits for them, and re-layouts  29 us (8%)
  matrix products  26.4 us (7%)
  other arithmetic  24.7 us (7%)
  starting transfers between devices  15.3 us (4%)
  between operations  14.2 us (4%)
    all_gather x1, waiting for transfers between devices, shards(): w_all = lax.all_gather(w_own, 'fs', axis=0, tiled=True)  97.7 us
    reduce_scatter x1, waiting for transfers between devices, shards(): own = lax.psum_scatter(grads, 'fs', scatter_dimension=0, tiled=True)  79.1 us
    psum x1, blocking collectives, shards(): tap_sum = lax.psum(tap_terms * factor, 'fs').reshape(3, 2, width)  35.4 us
    ppermute x4, waiting for transfers between devices, shift(): lax.ppermute(x, axis, [(i, (i + step) % count) for i in range(count)])  24.4 us
    dynamic_update_slice x4, local copies, waits for them, and re-layouts, shards(): cols = lax.dynamic_update_slice_in_dim(cols, new, place, 1)  15 us
    ppermute x2, waiting for transfers between devices, with_halo(): lax.ppermute(rows[rows.shape[0] - HALO:], 'fs', [(i, i + 1) for i in rang...  9.85 us
    ppermute x2, starting transfers between devices, with_halo(): lax.ppermute(rows[rows.shape[0] - HALO:], 'fs', [(i, i + 1) for i in rang...  9.6 us
    dot_general x1, matrix products, shards(): lax.dot_general(pre_cot, w_all, contract_cols, preferred_element_type=jnp...  9.31 us
  transfers between devices with their start and end apart: 12, of which 7 were waited for; matrix products, arithmetic and copies ran while one was open for 12% of the time, Pallas kernels for 0%

commit v1 on v0

--- a/solution.py
+++ b/solution.py
@@ -4,6 +4,17 @@
 from jax.sharding import PartitionSpec as P
 
 HALO = 8
+
+
+def turned_line(x, axis, dim):
+    n_dev = lax.axis_size(axis)
+    right = [(i, (i + 1) % n_dev) for i in range(n_dev)]
+    parts = [x]
+    for stride in range(1, n_dev):
+        parts = [lax.ppermute(parts[0], axis, right), *parts]
+    result = jnp.concatenate(parts, axis=dim)
+    places = (lax.axis_index(axis) + 1) * parts[-1].shape[dim]
+    return jnp.roll(result, places, axis=dim)
 
 
 def shift(x, axis, step):
@@ -53,7 +64,7 @@
         ],
         axis=1,
     )
-    w_all = lax.all_gather(w_own, "fs", axis=0, tiled=True)
+    w_all = turned_line(w_own, "fs", 0)
     x_ext = with_halo(inputs[0])
     g_ext = with_halo(out_grad[0])
     x_blocks, g_blocks = ([x_ext], [part_cols(g_ext, rep)])

time: 369 us -> 379 us (1.027)
  local copies, waits for them, and re-layouts: 29 us -> 40.6 us
  starting transfers between devices: 15.3 us -> 19.3 us
  waiting for transfers between devices: 217 us -> 213 us
    all_gather x1 -> x0, waiting for transfers between devices: 97.7 us -> none  [shards(): w_all = lax.all_gather(w_own, 'fs', axis=0, tiled=True)]
    ppermute x0 -> x7, waiting for transfers between devices: none -> 77.9 us  [turned_line(): parts = [lax.ppermute(parts[0], axis, right), *parts]]
    ppermute x2, waiting for transfers between devices: 9.85 us -> 28.2 us  [with_halo(): lax.ppermute(rows[rows.shape[0] - HALO:], 'fs', [(i, i + 1) for i in rang...]
    unnamed x9 -> x31, local copies, waits for them, and re-layouts: 1.53 us -> 10.3 us
    ppermute x0 -> x7, starting transfers between devices: none -> 5.05 us  [turned_line(): parts = [lax.ppermute(parts[0], axis, right), *parts]]
  transfers between devices with their start and end apart: 12 -> 18, of which waited for: 7 -> 11; matrix products, arithmetic and copies ran while one was open for 12% -> 15% of each run, Pallas kernels for 0% -> 0%
where the time goes in v1:
time: 379 us; the launch traced here: 378 us
  waiting for transfers between devices  213 us (56%)
  local copies, waits for them, and re-layouts  40.6 us (11%)
  blocking collectives  40.4 us (11%)
  other arithmetic  27.2 us (7%)
  matrix products  23.6 us (6%)
  starting transfers between devices  19.3 us (5%)
  between operations  14.3 us (4%)
    reduce_scatter x1, waiting for transfers between devices, shards(): own = lax.psum_scatter(grads, 'fs', scatter_dimension=0, tiled=True)  79.2 us
    ppermute x7, waiting for transfers between devices, turned_line(): parts = [lax.ppermute(parts[0], axis, right), *parts]  77.9 us
    psum x1, blocking collectives, shards(): tap_sum = lax.psum(tap_terms * factor, 'fs').reshape(3, 2, width)  34.2 us
    ppermute x2, waiting for transfers between devices, with_halo(): lax.ppermute(rows[rows.shape[0] - HALO:], 'fs', [(i, i + 1) for i in rang...  28.2 us
    ppermute x4, waiting for transfers between devices, shift(): lax.ppermute(x, axis, [(i, (i + step) % count) for i in range(count)])  22.8 us
    dynamic_update_slice x4, local copies, waits for them, and re-layouts, shards(): cols = lax.dynamic_update_slice_in_dim(cols, new, place, 1)  15 us
    unnamed x31, local copies, waits for them, and re-layouts  10.3 us
    dot_general x1, matrix products, shards(): lax.dot_general(pre_cot, w_all, contract_cols, preferred_element_type=jnp...  9.22 us
  transfers between devices with their start and end apart: 18, of which 11 were waited for; matrix products, arithmetic and copies ran while one was open for 15% of the time, Pallas kernels for 0%

profile of v1, /device:TPU:2, one launch (start us, length us, event | category | flops | bytes accessed | tf_op | source)
XLA Modules:
  0.0 378.1 jit_solution(14543180809324768747)
XLA Ops:
  8.8 1.6 collective-permute-start.6
  10.4 20.6 %collective-permute-done.6 = bf16[256,1536]{1,0:T(8,128)(2,1)S(1)} collective-permute-done((bf16[256,1536]{1,0:T(8,128)(2,1)S(1)}, bf16[256,1536]{1,0:T(8,128)(2,1)S(1)}, u32[]{:S(2)}, u32[]{:S(2)}) %collective-permute-start.6) | collective-permute-done | bytes 786464 | tf_op jit(solution)/shard_map/ppermute | solution.py:14
  31.0 1.8 copy.18
  32.9 3.5 collective-permute-start.4
  37.6 20.9 %collective-permute-done.4 = bf16[8,1024]{0,1:T(8,128)(2,1)} collective-permute-done((bf16[8,1024]{0,1:T(8,128)(2,1)S(1)}, bf16[8,1024]{0,1:T(8,128)(2,1)}, u32[]{:S(2)}, u32[]{:S(2)}) %collective-permute-start.4) | collective-permute-done | bytes 16416 | tf_op jit(solution)/shard_map/ppermute | solution.py:28
  62.3 2.6 collective-permute-start.8
  66.1 15.2 %collective-permute-done.5 = bf16[400,1024]{1,0:T(8,128)(2,1)} collective-permute-done((bf16[400,1024]{1,0:T(8,128)(2,1)}, bf16[400,1024]{1,0:T(8,128)(2,1)}, u32[]{:S(2)}, u32[]{:S(2)}) %collective-permute-start.5) | collective-permute-done | bytes 819232 | tf_op jit(solution)/shard_map/ppermute | solution.py:22
  84.7 1.6 pad_maximum_fusion.4
  86.4 18.1 %collective-permute-done.9 = bf16[256,1536]{1,0:T(8,128)(2,1)} collective-permute-done((bf16[256,1536]{1,0:T(8,128)(2,1)}, bf16[256,1536]{1,0:T(8,128)(2,1)}, u32[]{:S(2)}, u32[]{:S(2)}) %collective-permute-start.9) | collective-permute-done | bytes 786464 | tf_op jit(solution)/shard_map/ppermute | solution.py:14
  104.4 19.6 %collective-permute-done.10 = bf16[256,1536]{1,0:T(8,128)(2,1)S(1)} collective-permute-done((bf16[256,1536]{1,0:T(8,128)(2,1)}, bf16[256,1536]{1,0:T(8,128)(2,1)S(1)}, u32[]{:S(2)}, u32[]{:S(2)}) %collective-permute-start.10) | collective-permute-done | bytes 786464 | tf_op jit(solution)/shard_map/ppermute | solution.py:14
  124.1 18.6 %collective-permute-done.11 = bf16[256,1536]{1,0:T(8,128)(2,1)S(1)} collective-permute-done((bf16[256,1536]{1,0:T(8,128)(2,1)S(1)}, bf16[256,1536]{1,0:T(8,128)(2,1)S(1)}, u32[]{:S(2)}, u32[]{:S(2)}) %collective-permute-start.11) | collective-permute-done | bytes 786464 | tf_op jit(solution)/shard_map/ppermute | solution.py:14
  143.4 3.4 collective-permute-start.1
  149.2 7.3 %collective-permute-done.1 = bf16[8,1408]{1,0:T(8,128)(2,1)S(1)} collective-permute-done((bf16[8,1408]{1,0:T(8,128)(2,1)S(1)}, bf16[8,1408]{1,0:T(8,128)(2,1)S(1)}, u32[]{:S(2)}, u32[]{:S(2)}) %collective-permute-start.1) | collective-permute-done | bytes 22560 | tf_op jit(solution)/shard_map/ppermute | solution.py:28
  156.5 4.4 %collective-permute-done = bf16[8,1408]{1,0:T(8,128)(2,1)S(1)} collective-permute-done((bf16[8,1408]{1,0:T(8,128)(2,1)S(1)}, bf16[8,1408]{1,0:T(8,128)(2,1)S(1)}, u32[]{:S(2)}, u32[]{:S(2)}) %collective-permute-start) | collective-permute-done | bytes 22560 | tf_op jit(solution)/shard_map/ppermute | solution.py:27
  165.1 6.1 %copy.23 = bf16[2,400,2048]{2,1,0:T(8,128)(2,1)} copy(bf16[2,400,2048]{1,2,0:T(8,128)(2,1)} %all-gather.3.cloned.1.call-done) | data formatting | bytes 6553600 | tf_op jit(solution)/shard_map/all_gather | solution.py:74
  179.1 5.5 %fusion.22 = bf16[800,1536]{1,0:T(8,128)(2,1)S(1)} fusion(bf16[800,2048]{1,0:T(8,128)(2,1)S(1)} %bitcast.53, bf16[4096,1536]{1,0:T(8,128)(2,1)S(1)} %constant_dynamic-update-slice_fusion, s32[]{:T(128)S(6)} %select_n.80), kind=kOutput, calls=%fused_computation.41 | convolution fusion | flops 5034393600 | bytes 12025860 | tf_op jit(solution)/shard_map/dot_general | solution.py:77
  186.6 1.7 fusion.7
  188.3 2.2 convert_multiply_fusion
  191.6 8.2 %fusion.19 = (f32[1536]{0:T(1024)S(1)}, f32[1536]{0:T(1024)S(1)}, f32[1536]{0:T(1024)S(1)}, bf16[2,384,1536]{2,1,0:T(8,128)(2,1)S(1)}) fusion(f32[2,400,1536]{2,1,0:T(8,128)S(1)} %convert.5, f32[2,400,768]{2,1,0:T(8,128)S(1)} %get-tuple-element.11, f32[2,400,768]{2,1,0:T(8,128)S(1)} %get-tuple-element.12, f32[2,399,1536]{2,1,0:T(8,128)S(1)} %get-tuple-element.18, ...), kind=kLoop, calls=%fused_computation.35 | loop fusion | flops 20049408 | bytes 31494144 | tf_op jit(solution)/shard_map/reduce_sum | solution.py:93
  199.9 9.2 %fusion.25 = bf16[768,2048]{1,0:T(8,128)(2,1)} fusion(bf16[768,1536]{1,0:T(8,128)(2,1)S(1)} %bitcast.54, bf16[4096,1536]{1,0:T(8,128)(2,1)} %copy-done.5, s32[]{:T(128)S(6)} %select_n.80), kind=kOutput, calls=%fused_computation.42 | convolution fusion | flops 4833411072 | bytes 11796484 | tf_op jit(solution)/shard_map/dot_general | solution.py:104
  209.4 8.9 %fusion = bf16[2048,1536]{1,0:T(8,128)(2,1)} fusion(bf16[2,384,1536]{2,1,0:T(8,128)(2,1)S(1)} %get-tuple-element.13, bf16[2,400,2048]{1,2,0:T(8,128)(2,1)} %all-gather.3.cloned.1.call-done), kind=kOutput, calls=%fused_computation.1 | convolution fusion | flops 4838129664 | bytes 11796480 | tf_op jit(solution)/shard_map/dot_general | solution.py:96
  218.5 34.2 %psum.7 = f32[1,3,2,768]{3,2,1,0:T(2,128)S(1)} all-reduce(f32[1,3,2,768]{3,2,1,0:T(2,128)S(1)} %all_gather_reshape.3), channel_id=1, replica_groups=mesh['rep'=2,'fs'=8,'tp'=2] {'fs'}, use_global_device_ids=true, to_apply=%region_5.6 | all-reduce | flops 4608 | bytes 36864 | tf_op jit(solution)/shard_map/psum | solution.py:128
  252.7 4.4 %all_gather.13 = f32[2,3,2,768]{3,2,1,0:T(2,128)S(1)} all-gather(f32[1,3,2,768]{3,2,1,0:T(2,128)S(1)} %psum.7), channel_id=1, replica_groups=mesh['rep'=2,'fs'=8,'tp'=2] {'rep'}, dimensions={0}, use_global_device_ids=true | all-gather | bytes 55296 | tf_op jit(solution)/shard_map/all_gather | solution.py:129
  257.1 1.8 all-gather
  260.2 1.7 collective-permute-start.13
  262.0 79.2 %reduce-scatter.5.cloned.1.call-done = bf16[256,1536]{1,0:T(8,128)(2,1)} async-done(((bf16[2048,1536]{1,0:T(8,128)(2,1)}), bf16[256,1536]{1,0:T(8,128)(2,1)}) %reduce-scatter.5.cloned.1.call-update) | async-done | bytes 786448 | tf_op jit(solution)/shard_map/reduce_scatter | solution.py:103
  342.4 2.3 fusion.30
  346.0 3.1 dynamic_update_slice.12
  349.2 3.1 dynamic_update_slice.14
  352.3 7.6 %collective-permute-done.14 = bf16[256,1536]{1,0:T(8,128)(2,1)S(1)} collective-permute-done((bf16[256,1536]{1,0:T(8,128)(2,1)}, bf16[256,1536]{1,0:T(8,128)(2,1)S(1)}, u32[]{:S(2)}, u32[]{:S(2)}) %collective-permute-start.14) | collective-permute-done | bytes 786464 | tf_op jit(solution)/shard_map/ppermute | solution.py:22
  360.4 4.4 %dynamic_update_slice.13 = bf16[256,1408]{1,0:T(8,128)(2,1)S(1)} dynamic-update-slice(bf16[256,1408]{1,0:T(8,128)(2,1)S(1)} %dynamic_update_slice.12, bf16[256,768]{1,0:T(8,128)(2,1)S(1)} %get-tuple-element.27, s32[]{:T(128)} %constant.64.clone.1, s32[]{:T(128)S(6)} %select_n.85) | dynamic-update-slice | bytes 786436 | tf_op jit(solution)/shard_map/dynamic_update_slice | solution.py:126
  366.0 4.3 %dynamic_update_slice.15 = bf16[256,1408]{1,0:T(8,128)(2,1)S(1)} dynamic-update-slice(bf16[256,1408]{1,0:T(8,128)(2,1)S(1)} %dynamic_update_slice.14, bf16[256,768]{1,0:T(8,128)(2,1)S(1)} %get-tuple-element.26, s32[]{:T(128)} %constant.64.clone.1, s32[]{:T(128)S(6)} %select_n.85) | dynamic-update-slice | bytes 786436 | tf_op jit(solution)/shard_map/dynamic_update_slice | solution.py:126
  (92 shorter events, 36.6 us)
Async XLA Ops:
  7.2 157.9 %all-gather.3.cloned.1.call-start = ((), (), s32[]{:S(2)}) async-start(), calls=%async_computation.2 | async-start | bytes 6291456 | tf_op jit(solution)/shard_map/all_gather | solution.py:74
  8.8 22.2 %collective-permute-start.6 = (bf16[256,1536]{1,0:T(8,128)(2,1)S(1)}, bf16[256,1536]{1,0:T(8,128)(2,1)S(1)}, u32[]{:S(2)}, u32[]{:S(2)}) collective-permute-start(bf16[256,1536]{1,0:T(8,128)(2,1)S(1)} %pad_maximum_fusion.8), channel_id=1, source_target_pairs={{0,2},{2,4},{4,6},{6,8},{8,10},{10,12},{12,14},{14,0},{1,3},{3,5},... | collective-permute-start | bytes 2359304 | tf_op jit(solution)/shard_map/ppermute | solution.py:14
  30.9 31.4 %copy-start.1 = (bf16[256,1536]{1,0:T(8,128)(2,1)}, bf16[256,1536]{1,0:T(8,128)(2,1)S(1)}, u32[]{:S(2)}) copy-start(bf16[256,1536]{1,0:T(8,128)(2,1)S(1)} %collective-permute-done.6) | copy-start | bytes 2359300
  31.0 31.4 %collective-permute-start.7 = (bf16[256,1536]{1,0:T(8,128)(2,1)S(1)}, bf16[256,1536]{1,0:T(8,128)(2,1)}, u32[]{:S(2)}, u32[]{:S(2)}) collective-permute-start(bf16[256,1536]{1,0:T(8,128)(2,1)S(1)} %collective-permute-done.6), channel_id=1, source_target_pairs={{0,2},{2,4},{4,6},{6,8},{8,10},{10,12},{12,14},{14,0},{1,3},{3,5},... | collective-permute-start | bytes 2359304 | tf_op jit(solution)/shard_map/ppermute | solution.py:14
  32.9 25.7 %collective-permute-start.4 = (bf16[8,1024]{0,1:T(8,128)(2,1)S(1)}, bf16[8,1024]{0,1:T(8,128)(2,1)}, u32[]{:S(2)}, u32[]{:S(2)}) collective-permute-start(bf16[8,1024]{0,1:T(8,128)(2,1)S(1)} %get-tuple-element.31), channel_id=1, source_target_pairs={{0,2},{2,4},{4,6},{6,8},{8,10},{10,12},{12,14},{1,3},{3,5},{5,7},{... | collective-permute-start | bytes 49160 | tf_op jit(solution)/shard_map/ppermute | solution.py:28
  36.3 22.2 %collective-permute-start.3 = (bf16[8,1024]{0,1:T(8,128)(2,1)S(1)}, bf16[8,1024]{0,1:T(8,128)(2,1)S(1)}, u32[]{:S(2)}, u32[]{:S(2)}) collective-permute-start(bf16[8,1024]{0,1:T(8,128)(2,1)S(1)} %get-tuple-element.30), channel_id=1, source_target_pairs={{2,0},{4,2},{6,4},{8,6},{10,8},{12,10},{14,12},{3,1},{5,3},{7,5},{... | collective-permute-start | bytes 49160 | tf_op jit(solution)/shard_map/ppermute | solution.py:27
  58.5 0.7 copy-start.4
  61.6 19.8 %collective-permute-start.5 = (bf16[400,1024]{1,0:T(8,128)(2,1)}, bf16[400,1024]{1,0:T(8,128)(2,1)}, u32[]{:S(2)}, u32[]{:S(2)}) collective-permute-start(bf16[400,1024]{1,0:T(8,128)(2,1)} %copy.21), channel_id=1, source_target_pairs={{0,16},{16,0},{1,17},{17,1},{2,18},{18,2},{3,19},{19,3},{4,20},{20... | collective-permute-start | bytes 2457608 | tf_op jit(solution)/shard_map/ppermute | solution.py:22
  62.3 21.5 %collective-permute-start.8 = (bf16[256,1536]{1,0:T(8,128)(2,1)}, bf16[256,1536]{1,0:T(8,128)(2,1)}, u32[]{:S(2)}, u32[]{:S(2)}) collective-permute-start(bf16[256,1536]{1,0:T(8,128)(2,1)} %collective-permute-done.7), channel_id=1, source_target_pairs={{0,2},{2,4},{4,6},{6,8},{8,10},{10,12},{12,14},{14,0},{1,3},{3,5},... | collective-permute-start | bytes 2359304 | tf_op jit(solution)/shard_map/ppermute | solution.py:14
  83.8 20.6 %collective-permute-start.9 = (bf16[256,1536]{1,0:T(8,128)(2,1)}, bf16[256,1536]{1,0:T(8,128)(2,1)}, u32[]{:S(2)}, u32[]{:S(2)}) collective-permute-start(bf16[256,1536]{1,0:T(8,128)(2,1)} %collective-permute-done.8), channel_id=1, source_target_pairs={{0,2},{2,4},{4,6},{6,8},{8,10},{10,12},{12,14},{14,0},{1,3},{3,5},... | collective-permute-start | bytes 2359304 | tf_op jit(solution)/shard_map/ppermute | solution.py:14
  86.3 172.7 %reduce-scatter.3.cloned.1.call-start = ((), (), s32[]{:S(2)}) async-start(), calls=%async_computation.3 | async-start | bytes 4718592 | tf_op jit(solution)/shard_map/reduce_scatter | solution.py:107
  104.4 19.6 %collective-permute-start.10 = (bf16[256,1536]{1,0:T(8,128)(2,1)}, bf16[256,1536]{1,0:T(8,128)(2,1)S(1)}, u32[]{:S(2)}, u32[]{:S(2)}) collective-permute-start(bf16[256,1536]{1,0:T(8,128)(2,1)} %collective-permute-done.9), channel_id=1, source_target_pairs={{0,2},{2,4},{4,6},{6,8},{8,10},{10,12},{12,14},{14,0},{1,3},{3,5},... | collective-permute-start | bytes 2359304 | tf_op jit(solution)/shard_map/ppermute | solution.py:14
  124.1 18.6 %collective-permute-start.11 = (bf16[256,1536]{1,0:T(8,128)(2,1)S(1)}, bf16[256,1536]{1,0:T(8,128)(2,1)S(1)}, u32[]{:S(2)}, u32[]{:S(2)}) collective-permute-start(bf16[256,1536]{1,0:T(8,128)(2,1)S(1)} %collective-permute-done.10), channel_id=1, source_target_pairs={{0,2},{2,4},{4,6},{6,8},{8,10},{10,12},{12,14},{14,0},{1,3},{3,5},... | collective-permute-start | bytes 2359304 | tf_op jit(solution)/shard_map/ppermute | solution.py:14
  142.7 28.5 %collective-permute-start.12 = (bf16[256,1536]{1,0:T(8,128)(2,1)S(1)}, bf16[256,1536]{1,0:T(8,128)(2,1)S(1)}, u32[]{:S(2)}, u32[]{:S(2)}) collective-permute-start(bf16[256,1536]{1,0:T(8,128)(2,1)S(1)} %collective-permute-done.11), channel_id=1, source_target_pairs={{0,2},{2,4},{4,6},{6,8},{8,10},{10,12},{12,14},{14,0},{1,3},{3,5},... | collective-permute-start | bytes 2359304 | tf_op jit(solution)/shard_map/ppermute | solution.py:14
  143.4 13.0 %collective-permute-start.1 = (bf16[8,1408]{1,0:T(8,128)(2,1)S(1)}, bf16[8,1408]{1,0:T(8,128)(2,1)S(1)}, u32[]{:S(2)}, u32[]{:S(2)}) collective-permute-start(bf16[8,1408]{1,0:T(8,128)(2,1)S(1)} %get-tuple-element.25), channel_id=1, source_target_pairs={{0,2},{2,4},{4,6},{6,8},{8,10},{10,12},{12,14},{1,3},{3,5},{5,7},{... | collective-permute-start | bytes 67592 | tf_op jit(solution)/shard_map/ppermute | solution.py:28
  146.8 14.0 %collective-permute-start = (bf16[8,1408]{1,0:T(8,128)(2,1)S(1)}, bf16[8,1408]{1,0:T(8,128)(2,1)S(1)}, u32[]{:S(2)}, u32[]{:S(2)}) collective-permute-start(bf16[8,1408]{1,0:T(8,128)(2,1)S(1)} %get-tuple-element.24), channel_id=1, source_target_pairs={{2,0},{4,2},{6,4},{8,6},{10,8},{12,10},{14,12},{3,1},{5,3},{7,5},{... | collective-permute-start | bytes 67592 | tf_op jit(solution)/shard_map/ppermute | solution.py:27
  163.8 24.5 %collective-permute-start.2 = (bf16[400,768]{1,0:T(8,128)(2,1)}, bf16[400,768]{1,0:T(8,128)(2,1)}, u32[]{:S(2)}, u32[]{:S(2)}) collective-permute-start(bf16[400,768]{1,0:T(8,128)(2,1)} %get-tuple-element.23), channel_id=1, source_target_pairs={{0,16},{16,0},{1,17},{17,1},{2,18},{18,2},{3,19},{19,3},{4,20},{20... | collective-permute-start | bytes 1843208 | tf_op jit(solution)/shard_map/ppermute | solution.py:22
  171.1 3.8 %copy-start.2 = (bf16[256,1536]{1,0:T(8,128)(2,1)S(1)}, bf16[256,1536]{1,0:T(8,128)(2,1)}, u32[]{:S(2)}) copy-start(bf16[256,1536]{1,0:T(8,128)(2,1)} %copy-done.1) | copy-start | bytes 2359300
  175.2 3.9 %copy-start = (bf16[2,400,2048]{2,1,0:T(8,128)(2,1)S(1)}, bf16[2,400,2048]{2,1,0:T(8,128)(2,1)}, u32[]{:S(2)}) copy-start(bf16[2,400,2048]{2,1,0:T(8,128)(2,1)} %copy.23) | copy-start | bytes 9830404
  179.1 5.5 %copy-start.5 = (bf16[4096,1536]{1,0:T(8,128)(2,1)}, bf16[4096,1536]{1,0:T(8,128)(2,1)S(1)}, u32[]{:S(2)}) copy-start(bf16[4096,1536]{1,0:T(8,128)(2,1)S(1)} %constant_dynamic-update-slice_fusion) | copy-start | bytes 37748740
  186.6 1.7 copy-start.3
  209.1 132.1 %reduce-scatter.5.cloned.1.call-start = ((), (), s32[]{:S(2)}) async-start(), calls=%async_computation.4 | async-start | bytes 7077888 | tf_op jit(solution)/shard_map/reduce_scatter | solution.py:103
  260.2 82.2 %collective-permute-start.13 = (bf16[384,1024]{1,0:T(8,128)(2,1)S(1)}, bf16[384,1024]{1,0:T(8,128)(2,1)S(1)}, u32[]{:S(2)}, u32[]{:S(2)}) collective-permute-start(bf16[384,1024]{1,0:T(8,128)(2,1)S(1)} %slice.184), channel_id=1, source_target_pairs={{0,16},{16,0},{1,17},{17,1},{2,18},{18,2},{3,19},{19,3},{4,20},{20... | collective-permute-start | bytes 2359304 | tf_op jit(solution)/shard_map/ppermute | solution.py:22
  341.2 18.7 %collective-permute-start.14 = (bf16[256,1536]{1,0:T(8,128)(2,1)}, bf16[256,1536]{1,0:T(8,128)(2,1)S(1)}, u32[]{:S(2)}, u32[]{:S(2)}) collective-permute-start(bf16[256,1536]{1,0:T(8,128)(2,1)} %reduce-scatter.5.cloned.1.call-done), channel_id=1, source_target_pairs={{0,16},{16,0},{1,17},{17,1},{2,18},{18,2},{3,19},{19,3},{4,20},{20... | collective-permute-start | bytes 2359304 | tf_op jit(solution)/shard_map/ppermute | solution.py:22
Sparse Core Ops, SparseCore 0:
  86.4 15.6 all-gather.2
  209.2 9.0 reduce-scatter.2
  221.9 119.2 reduce-scatter.4
